TPU v7x, 32 devices: a whole 2x2x4 slice. The times are simulated.
32 devices in a mesh: sp: 8 (over z, x), tp: 4 (over y, core).
Axes of the slice: x: 2, y: 2, z: 4, core: 2. Of those that a mesh axis runs over, the one named last changes fastest.
Arguments:
- queries: bfloat16 [8192, 2048], P('sp', 'tp'), may hold values from -16 to 16
- key_rows: bfloat16 [8192, 512], P('sp', 'tp'), may hold values from -16 to 16
- value_rows: bfloat16 [8192, 512], P('sp', 'tp'), may hold values from -6 to 6
- doc_ids: int32 [8192], P('sp'), may hold values from 0 to 3, never falling along the last dimension, each value on 1 to 4096 neighbouring positions
- sink_logit: float32 [32], P('tp'), may hold values from 3 to 7
- residual: bfloat16 [8192, 2048], P(('sp', 'tp')), may hold values from -6 to 6
- out_weight: bfloat16 [2048, 2048], P('tp'), may hold values from -3.5 to 3.5
- norm_gain: float32 [2048], replicated, may hold values from 0.1 to 1.9
- gate_weight: bfloat16 [8, 2048, 512], P('sp'), may hold values from -0.125 to 0.125
- up_weight: bfloat16 [8, 2048, 512], P('sp'), may hold values from -0.125 to 0.125
- down_weight: bfloat16 [8, 512, 2048], P('sp'), may hold values from -0.25 to 0.25
- routes: int32 [8192, 2], P(('sp', 'tp')), may hold values from 0 to 7, as said below
- route_weights: float32 [8192, 2], P(('sp', 'tp')), may hold values from 0.2 to 0.8
Outputs:
- mixed: bfloat16 [8192, 2048], P(('sp', 'tp'))
Inputs may be any that keep to these rules, and one draw needn't show every extreme that they name: `doc_ids`: never falls along the positions. `routes`: each aligned block of 256 rows names every expert exactly 64 times; the experts of one row differ and lie in one group of 2 consecutive numbers.
All inputs are finite; a program needn't handle non-finite values.
Results may differ from a plain program's by a relative error of at most 0.012.
Values may be sent and summed in bfloat16 or wider, within the bound.
A program may use at most 128 MiB of HBM per device.

v0:
```python
import jax
import jax.numpy as jnp
from jax import lax
from jax.sharding import PartitionSpec as P

HD = 64
WINDOW = 128
neg_fill = -1e30
eps_norm = 1e-06


def extended(block, sides, width):
    for axis, dim in sides:
        count = lax.axis_size(axis)
        forward = [(i, i + 1) for i in range(count - 1)]
        backward = [(target, source) for source, target in forward]
        low = lax.ppermute(
            lax.slice_in_dim(block, block.shape[dim] - width, None, axis=dim), axis, forward
        )
        high = lax.ppermute(lax.slice_in_dim(block, 0, width, axis=dim), axis, backward)
        block = jnp.concatenate([low, block, high], axis=dim)
    return block


def attend(
    query_part,
    key_part,
    value_part,
    query_docs,
    key_docs,
    query_start,
    key_start,
    sink_logit,
    extent,
):
    query_count = query_part.shape[0]
    key_count = key_part.shape[0]
    groups = key_part.shape[1] // HD
    head_ratio = sink_logit.shape[0] // groups
    query_heads = query_part.reshape(query_count, groups, head_ratio, HD)
    key_heads = key_part.reshape(key_count, groups, HD)
    value_heads = value_part.reshape(key_count, groups, HD)
    scores = jnp.einsum(
        "qgrd,kgd->grqk", query_heads, key_heads, preferred_element_type=jnp.float32
    ) * HD ** (-0.5)
    query_pos = query_start + jnp.arange(query_count, dtype=jnp.int32)
    key_pos = key_start + jnp.arange(key_count, dtype=jnp.int32)
    inside = (key_pos >= 0) & (key_pos < extent)
    allowed = (
        (jnp.abs(query_pos[:, None] - key_pos[None, :]) <= WINDOW)
        & (query_docs[:, None] == key_docs[None, :])
        & inside[None, :]
    )
    masked = jnp.where(allowed[None, None], scores, neg_fill)
    sink_col = sink_logit.reshape(groups, head_ratio)[:, :, None, None]
    row_top = jnp.maximum(jnp.max(masked, axis=3, keepdims=True), sink_col)
    exponent = jnp.where(allowed[None, None], jnp.exp(masked - row_top), 0.0)
    denominator = jnp.sum(exponent, axis=3, keepdims=True) + jnp.exp(sink_col - row_top)
    attn_weight = (exponent / denominator).astype(jnp.bfloat16)
    attended = jnp.einsum(
        "grqk,kgd->qgrd", attn_weight, value_heads, preferred_element_type=jnp.float32
    )
    return attended.astype(jnp.bfloat16).reshape(query_count, -1)


def fetch_margins(key_rows, value_rows, doc_float):
    return (
        extended(key_rows, (("sp", 0),), WINDOW),
        extended(value_rows, (("sp", 0),), WINDOW),
        extended(doc_float, (("sp", 0),), WINDOW),
    )


def per_device(
    queries,
    key_rows,
    value_rows,
    doc_ids,
    sink_logit,
    residual,
    out_weight,
    norm_gain,
    gate_weight,
    up_weight,
    down_weight,
    routes,
    route_weights,
):
    local_rows = queries.shape[0]
    anchor = lax.axis_index("sp") * local_rows
    extent = local_rows * lax.axis_size("sp")
    doc_float = doc_ids.astype(jnp.bfloat16)
    block_rows = min(512, local_rows)
    padded_keys, padded_values, padded_docs = fetch_margins(key_rows, value_rows, doc_float)
    block_parts = []
    for row_start in range(0, local_rows, block_rows):
        key_end = row_start + block_rows + 2 * WINDOW
        block_parts.append(
            attend(
                queries[row_start : row_start + block_rows],
                padded_keys[row_start:key_end],
                padded_values[row_start:key_end],
                doc_float[row_start : row_start + block_rows],
                padded_docs[row_start:key_end],
                anchor + row_start,
                anchor + row_start - WINDOW,
                sink_logit,
                extent,
            )
        )
    attended = jnp.concatenate(block_parts, axis=0)
    regrouped = lax.all_to_all(attended, "tp", split_axis=0, concat_axis=1, tiled=True)
    shard_rows = out_weight.shape[0]
    initial = jnp.zeros((regrouped.shape[0], out_weight.shape[1]), jnp.float32)
    running = initial
    weight_piece = lax.all_gather(out_weight, "tp", axis=0, tiled=True)
    for shard_index in range(weight_piece.shape[0] // shard_rows):
        columns = lax.dynamic_slice_in_dim(regrouped, shard_index * shard_rows, shard_rows, 1)
        partial_value = jnp.dot(
            columns,
            weight_piece[shard_index * shard_rows : (shard_index + 1) * shard_rows],
            preferred_element_type=jnp.float32,
        )
        running = running + partial_value.astype(jnp.bfloat16).astype(jnp.float32)
    stream = (residual.astype(jnp.float32) + running).astype(jnp.bfloat16)
    stream_f = stream.astype(jnp.float32)
    scale = lax.rsqrt(jnp.mean(stream_f * stream_f, axis=1, keepdims=True) + eps_norm)
    normed = (stream_f * scale * norm_gain[None, :]).astype(jnp.bfloat16)
    home_rows = normed.shape[0]
    width = normed.shape[1]
    route_count = routes.shape[1]
    expert_count = lax.axis_size("sp") * gate_weight.shape[0]
    capacity = route_count * home_rows // expert_count
    flat_routes = routes.reshape(-1)
    one_hot = (flat_routes[:, None] == jnp.arange(expert_count, dtype=jnp.int32)[None, :]).astype(
        jnp.int32
    )
    earlier = jnp.cumsum(one_hot, axis=0) - one_hot
    slot_rank = jnp.sum(earlier * one_hot, axis=1)
    slot_index = flat_routes * capacity + slot_rank
    source_row = (
        jnp.zeros((expert_count * capacity,), jnp.int32)
        .at[slot_index]
        .set(jnp.arange(home_rows * route_count, dtype=jnp.int32) // route_count)
    )
    outgoing = normed[source_row].reshape(expert_count, capacity, width)
    incoming = lax.all_to_all(outgoing, "sp", split_axis=0, concat_axis=0, tiled=True)
    flat_rows = incoming.reshape(-1, width)
    gate_act = jnp.dot(flat_rows, gate_weight[0], preferred_element_type=jnp.float32)
    up_act = jnp.dot(flat_rows, up_weight[0], preferred_element_type=jnp.float32)
    hidden = (jax.nn.silu(gate_act) * up_act).astype(jnp.bfloat16)
    produced = jnp.dot(hidden, down_weight[0], preferred_element_type=jnp.float32).astype(
        jnp.bfloat16
    )
    returned = lax.all_to_all(
        produced.reshape(incoming.shape), "sp", split_axis=0, concat_axis=0, tiled=True
    )
    route_out = returned.reshape(-1, width)[slot_index].reshape(home_rows, route_count, width)
    weighted = jnp.sum(route_weights[:, :, None] * route_out.astype(jnp.float32), axis=1)
    return (stream_f + weighted).astype(jnp.bfloat16)


def solution(mesh):
    return jax.shard_map(
        per_device,
        mesh=mesh,
        in_specs=(
            P("sp", "tp"),
            P("sp", "tp"),
            P("sp", "tp"),
            P("sp"),
            P("tp"),
            P(("sp", "tp"), None),
            P("tp", None),
            P(),
            P("sp", None, None),
            P("sp", None, None),
            P("sp", None, None),
            P(("sp", "tp"), None),
            P(("sp", "tp"), None),
        ),
        out_specs=P(("sp", "tp"), None),
        check_vma=False,
    )
```

profile of v0, /device:TPU:0, one launch (start us, length us, event | category | flops | bytes accessed | tf_op | source)
XLA Modules:
  0.0 266.3 jit_solution(878454835703081858)
XLA Ops:
  8.0 4.9 %collective-permute-start.1 = (bf16[128]{0:T(256)(128)(2,1)S(1)}, bf16[128]{0:T(256)(128)(2,1)S(1)}, u32[]{:S(2)}, u32[]{:S(2)}) collective-permute-start(bf16[128]{0:T(256)(128)(2,1)S(1)} %get-tuple-element.17), channel_id=1, source_target_pairs={{0,4},{4,8},{8,12},{12,16},{16,20},{20,24},{24,28},{1,5},{5,9},{9,... | collective-permute-start | bytes 776 | tf_op jit(solution)/shard_map/ppermute | solution.py:17
  14.1 1.4 fusion.63
  15.5 4.5 %collective-permute-start.2 = (bf16[128,128]{1,0:T(8,128)(2,1)}, bf16[128,128]{1,0:T(8,128)(2,1)S(1)}, u32[]{:S(2)}, u32[]{:S(2)}) collective-permute-start(bf16[128,128]{1,0:T(8,128)(2,1)} %get-tuple-element.9), channel_id=1, source_target_pairs={{0,4},{4,8},{8,12},{12,16},{16,20},{20,24},{24,28},{1,5},{5,9},{9,... | collective-permute-start | bytes 98312 | tf_op jit(solution)/shard_map/ppermute | solution.py:17
  21.4 1.4 fusion.64
  22.8 5.0 %collective-permute-start = (bf16[128,128]{1,0:T(8,128)(2,1)}, bf16[128,128]{1,0:T(8,128)(2,1)S(1)}, u32[]{:S(2)}, u32[]{:S(2)}) collective-permute-start(bf16[128,128]{1,0:T(8,128)(2,1)} %get-tuple-element.13), channel_id=1, source_target_pairs={{0,4},{4,8},{8,12},{12,16},{16,20},{20,24},{24,28},{1,5},{5,9},{9,... | collective-permute-start | bytes 98312 | tf_op jit(solution)/shard_map/ppermute | solution.py:17
  41.6 2.4 fusion.30
  44.0 1.8 pad_maximum_fusion.3
  45.7 1.7 copy.36
  47.5 1.7 copy.40
  49.2 1.8 pad_maximum_fusion.4
  51.0 1.7 copy.35
  52.8 3.1 %fusion = (f32[2,4,512]{2,1,0:T(4,128)S(1)}, f32[2,768,512,4]{2,1,3,0:T(8,128)S(1)}) fusion(pred[512,768]{0,1:T(8,128)(4,1)S(1)} %get-tuple-element.30, bf16[768,2,64,1]{0,2,3,1:T(8,128)(2,1)} %bitcast.107, bf16[512,2,4,64]{0,3,2,1:T(8,128)(2,1)S(1)} %bitcast.104), kind=kOutput, calls=%fused_computation.9 | convolution fusion | flops 412086272 | bytes 13713408 | tf_op jit(solution)/shard_map/qgrd,kgd->grqk/dot_general | solution.py:43
  55.9 6.6 %fusion.1 = (f32[2,4,512]{2,1,0:T(4,128)S(1)}, f32[2,768,512,4]{2,1,3,0:T(8,128)}) fusion(pred[512,768]{0,1:T(8,128)(4,1)S(1)} %get-tuple-element.29, bf16[768,2,64,1]{0,2,3,1:T(8,128)(2,1)S(1)} %bitcast.106, bf16[512,2,4,64]{0,3,2,1:T(8,128)(2,1)S(1)} %bitcast.105), kind=kOutput, calls=%fused_computation.10 | convolution fusion | flops 412086272 | bytes 13713408 | tf_op jit(solution)/shard_map/qgrd,kgd->grqk/dot_general | solution.py:43
  62.5 3.1 %fusion.2 = f32[2,4,512]{2,1,0:T(4,128)S(1)} fusion(f32[2,768,512,4]{2,1,3,0:T(8,128)S(1)} %get-tuple-element.24, f32[2,4,512]{2,1,0:T(4,128)S(1)} %broadcast_maximum_fusion.1, pred[512,768]{0,1:T(8,128)(4,1)S(1)} %get-tuple-element.30), kind=kLoop, calls=%fused_computation.11 | loop fusion | flops 15724544 | bytes 13008896 | tf_op jit(solution)/shard_map/reduce_sum | solution.py:58
  65.7 4.7 %fusion.39 = bf16[2,64,4,512]{3,1,2,0:T(8,128)(2,1)} fusion(bf16[768,2,64,1]{0,2,3,1:T(8,128)(2,1)S(1)} %bitcast.110, f32[2,768,512,4]{2,1,3,0:T(8,128)S(1)} %get-tuple-element.24, f32[2,4,512]{2,1,0:T(4,128)S(1)} %get-tuple-element.21, f32[2,4,512]{2,1,0:T(4,128)S(1)} %broadcast_maximum_fusion.1, pred[512,768]{0,1:T(8,128)(4,1)S(1)} %get-tuple-element.30), kind=kOutput, calls=%fused_computation.55 | convolution fusion | flops 421789696 | bytes 13729792 | tf_op jit(solution)/shard_map/grqk,kgd->qgrd/dot_general | solution.py:60
  71.8 6.8 %fusion.3 = f32[2,4,512]{2,1,0:T(4,128)S(1)} fusion(f32[2,768,512,4]{2,1,3,0:T(8,128)} %get-tuple-element.26, f32[2,4,512]{2,1,0:T(4,128)S(1)} %get-tuple-element.22, pred[512,768]{0,1:T(8,128)(4,1)S(1)} %get-tuple-element.29), kind=kLoop, calls=%fused_computation.12 | loop fusion | flops 15724544 | bytes 13008896 | tf_op jit(solution)/shard_map/reduce_sum | solution.py:58
  80.1 4.6 %fusion.38 = bf16[2,64,4,512]{3,1,2,0:T(8,128)(2,1)} fusion(bf16[768,2,64,1]{0,2,3,1:T(8,128)(2,1)S(1)} %bitcast.111, f32[2,768,512,4]{2,1,3,0:T(8,128)S(1)} %copy-done.1, f32[2,4,512]{2,1,0:T(4,128)S(1)} %exponential_add_fusion, f32[2,4,512]{2,1,0:T(4,128)S(1)} %get-tuple-element.22, pred[512,768]{0,1:T(8,128)(4,1)S(1)} %get-tuple-element.29), kind=kOutput, calls=%fused_computation.54 | convolution fusion | flops 421789696 | bytes 13729792 | tf_op jit(solution)/shard_map/grqk,kgd->qgrd/dot_general | solution.py:60
  87.0 3.8 %all-to-all-start = ((bf16[4,256,512]{2,1,0:T(8,128)(2,1)}), bf16[4,256,512]{2,1,0:T(8,128)(2,1)S(1)}, u32[]{:S(2)}, u32[]{:S(2)}) async-start(bf16[4,256,512]{2,1,0:T(8,128)(2,1)} %bitcast.100), calls=%async_computation | async-start | bytes 2097152 | tf_op jit(solution)/shard_map/all_to_all | solution.py:112
  91.0 2.4 scatter_custom_fusion
  93.4 11.6 %all-to-all-done = bf16[4,256,512]{2,1,0:T(8,128)(2,1)S(1)} async-done(((bf16[4,256,512]{2,1,0:T(8,128)(2,1)}), bf16[4,256,512]{2,1,0:T(8,128)(2,1)S(1)}, u32[]{:S(2)}, u32[]{:S(2)}) %all-to-all-start) | async-done | bytes 1048608 | tf_op jit(solution)/shard_map/all_to_all | solution.py:112
  106.0 1.5 copy.45
  107.5 2.5 fusion.12
  110.0 2.9 %fusion.13 = f32[256,2048]{1,0:T(8,128)S(1)} fusion(bf16[2048,2048]{1,0:T(8,128)(2,1)} %all-gather.2.cloned.1.call-done, bf16[256,2048]{0,1:T(8,128)(2,1)S(1)} %bitcast.96), kind=kOutput, calls=%fused_computation.31 | convolution fusion | flops 537919488 | bytes 4456448 | tf_op jit(solution)/shard_map/dot_general | solution.py:119
  116.6 3.3 %gather_fusion = bf16[512,2048]{1,0:T(8,128)(2,1)} fusion(bf16[256,2048]{1,0:T(8,128)(2,1)S(1)} %fusion.17, s32[1024]{0:T(1024)S(1)} %pad_clamp_fusion.1), kind=kCustom, calls=%fused_computation | custom fusion | bytes 4196352 | tf_op jit(solution)/shard_map/gather | solution.py:146
  119.9 56.4 %all_to_all.29 = bf16[8,64,2048]{2,1,0:T(8,128)(2,1)S(1)} all-to-all(bf16[8,64,2048]{2,1,0:T(8,128)(2,1)} %bitcast.94), channel_id=1, replica_groups=mesh['sp'=8,'tp'=4] {'sp'}, dimensions={0} | all-to-all | bytes 4194304 | tf_op jit(solution)/shard_map/all_to_all | solution.py:147
  176.3 1.3 copy-done.6
  178.9 6.0 %convolution_convert_fusion = bf16[512,2048]{1,0:T(8,128)(2,1)} fusion(bf16[1,512,2048]{2,1,0:T(8,128)(2,1)S(1)} %copy-done, bf16[512,2048]{1,0:T(8,128)(2,1)} %bitcast.103, bf16[1,2048,512]{2,1,0:T(8,128)(2,1)} %param.22, f32[512,512]{1,0:T(8,128)S(1)} %fusion.26), kind=kOutput, calls=%fused_computation.19 | convolution fusion | flops 2150105088 | bytes 9437184 | tf_op jit(solution)/shard_map/dot_general | solution.py:152
  184.9 4.7 %all-to-all-start.2 = ((bf16[8,64,2048]{2,1,0:T(8,128)(2,1)}), bf16[8,64,2048]{2,1,0:T(8,128)(2,1)}, u32[]{:S(2)}, u32[]{:S(2)}) async-start(bf16[8,64,2048]{2,1,0:T(8,128)(2,1)} %bitcast.101), calls=%async_computation.2 | async-start | bytes 4194304 | tf_op jit(solution)/shard_map/all_to_all | solution.py:155
  189.8 46.9 %all-to-all-done.2 = bf16[8,64,2048]{2,1,0:T(8,128)(2,1)} async-done(((bf16[8,64,2048]{2,1,0:T(8,128)(2,1)}), bf16[8,64,2048]{2,1,0:T(8,128)(2,1)}, u32[]{:S(2)}, u32[]{:S(2)}) %all-to-all-start.2) | async-done | bytes 2097184 | tf_op jit(solution)/shard_map/all_to_all | solution.py:155
  236.7 7.1 %gather_fusion.1 = bf16[512,2048]{1,0:T(8,128)(2,1)} fusion(bf16[512,2048]{1,0:T(8,128)(2,1)} %bitcast.33, s32[1024]{0:T(1024)S(1)} %pad_clamp_fusion), kind=kCustom, calls=%fused_computation.1 | custom fusion | bytes 4196352 | tf_op jit(solution)/shard_map/gather | solution.py:158
  243.8 5.4 %reshape.312 = f32[256,2,2048]{2,1,0:T(2,128)} reshape(bf16[512,2048]{1,0:T(8,128)(2,1)} %gather_fusion.1) | data formatting | bytes 6291456 | tf_op jit(solution)/shard_map/convert_element_type | solution.py:159
  249.2 9.0 %multiply_reduce_fusion = f32[256,2048]{1,0:T(8,128)S(1)} fusion(f32[256,2,2048]{2,1,0:T(2,128)} %reshape.312, f32[256,2]{1,0:T(8,128)S(1)} %copy.46), kind=kLoop, calls=%fused_computation.15 | loop fusion | flops 1572864 | bytes 6293504 | tf_op jit(solution)/shard_map/reduce_sum | solution.py:159
  (107 shorter events, 30.5 us)
Async XLA Ops:
  6.5 172.4 %copy-start = (bf16[1,512,2048]{2,1,0:T(8,128)(2,1)S(1)}, bf16[1,512,2048]{2,1,0:T(8,128)(2,1)}, u32[]{:S(2)}) copy-start(bf16[1,512,2048]{2,1,0:T(8,128)(2,1)} %param.23) | copy-start | bytes 6291460
  6.5 21.2 %copy-start.18 = (s32[256,2]{0,1:T(2,128)S(1)}, s32[256,2]{0,1:T(2,128)}, u32[]{:S(2)}) copy-start(s32[256,2]{0,1:T(2,128)} %param.24) | copy-start | bytes 6148
  6.5 101.0 %all-gather.2.cloned.1.call-start = ((), (), s32[]{:S(2)}) async-start(), calls=%async_computation.3 | async-start | bytes 10485760 | tf_op jit(solution)/shard_map/all_gather | solution.py:116
  7.4 23.7 %copy-start.24 = (f32[8]{0:T(128)S(1)}, f32[8]{0:T(128)}, u32[]{:S(2)}) copy-start(f32[8]{0:T(128)} %param.17) | copy-start | bytes 100
  7.4 30.7 %copy-start.13 = (bf16[1024]{0:T(1024)(128)(2,1)}, bf16[1024]{0:T(1024)(128)(2,1)S(1)}, u32[]{:S(2)}) copy-start(bf16[1024]{0:T(1024)(128)(2,1)S(1)} %convert_element_type.80) | copy-start | bytes 6148
  8.0 31.1 %collective-permute-start.1 = (bf16[128]{0:T(256)(128)(2,1)S(1)}, bf16[128]{0:T(256)(128)(2,1)S(1)}, u32[]{:S(2)}, u32[]{:S(2)}) collective-permute-start(bf16[128]{0:T(256)(128)(2,1)S(1)} %get-tuple-element.17), channel_id=1, source_target_pairs={{0,4},{4,8},{8,12},{12,16},{16,20},{20,24},{24,28},{1,5},{5,9},{9,... | collective-permute-start | bytes 776 | tf_op jit(solution)/shard_map/ppermute | solution.py:17
  12.8 28.0 %collective-permute-start.4 = (bf16[128]{0:T(256)(128)(2,1)}, bf16[128]{0:T(256)(128)(2,1)}, u32[]{:S(2)}, u32[]{:S(2)}) collective-permute-start(bf16[128]{0:T(256)(128)(2,1)} %get-tuple-element.18), channel_id=1, source_target_pairs={{4,0},{8,4},{12,8},{16,12},{20,16},{24,20},{28,24},{5,1},{9,5},{13... | collective-permute-start | bytes 776 | tf_op jit(solution)/shard_map/ppermute | solution.py:20
  15.5 28.4 %collective-permute-start.2 = (bf16[128,128]{1,0:T(8,128)(2,1)}, bf16[128,128]{1,0:T(8,128)(2,1)S(1)}, u32[]{:S(2)}, u32[]{:S(2)}) collective-permute-start(bf16[128,128]{1,0:T(8,128)(2,1)} %get-tuple-element.9), channel_id=1, source_target_pairs={{0,4},{4,8},{8,12},{12,16},{16,20},{20,24},{24,28},{1,5},{5,9},{9,... | collective-permute-start | bytes 98312 | tf_op jit(solution)/shard_map/ppermute | solution.py:17
  20.1 23.9 %collective-permute-start.5 = (bf16[128,128]{1,0:T(8,128)(2,1)}, bf16[128,128]{1,0:T(8,128)(2,1)S(1)}, u32[]{:S(2)}, u32[]{:S(2)}) collective-permute-start(bf16[128,128]{1,0:T(8,128)(2,1)} %get-tuple-element.10), channel_id=1, source_target_pairs={{4,0},{8,4},{12,8},{16,12},{20,16},{24,20},{28,24},{5,1},{9,5},{13... | collective-permute-start | bytes 98312 | tf_op jit(solution)/shard_map/ppermute | solution.py:20
  22.8 26.5 %collective-permute-start = (bf16[128,128]{1,0:T(8,128)(2,1)}, bf16[128,128]{1,0:T(8,128)(2,1)S(1)}, u32[]{:S(2)}, u32[]{:S(2)}) collective-permute-start(bf16[128,128]{1,0:T(8,128)(2,1)} %get-tuple-element.13), channel_id=1, source_target_pairs={{0,4},{4,8},{8,12},{12,16},{16,20},{20,24},{24,28},{1,5},{5,9},{9,... | collective-permute-start | bytes 98312 | tf_op jit(solution)/shard_map/ppermute | solution.py:17
  38.1 14.7 %copy-start.7 = (bf16[512,512]{0,1:T(8,128)(2,1)S(1)}, bf16[512,512]{0,1:T(8,128)(2,1)}, u32[]{:S(2)}) copy-start(bf16[512,512]{0,1:T(8,128)(2,1)} %copy.37) | copy-start | bytes 1572868
  39.5 9.7 %collective-permute-start.3 = (bf16[128,128]{1,0:T(8,128)(2,1)}, bf16[128,128]{1,0:T(8,128)(2,1)S(1)}, u32[]{:S(2)}, u32[]{:S(2)}) collective-permute-start(bf16[128,128]{1,0:T(8,128)(2,1)} %get-tuple-element.14), channel_id=1, source_target_pairs={{4,0},{8,4},{12,8},{16,12},{20,16},{24,20},{28,24},{5,1},{9,5},{13... | collective-permute-start | bytes 98312 | tf_op jit(solution)/shard_map/ppermute | solution.py:20
  52.8 3.1 %copy-start.15 = (f32[2,4]{1,0:T(2,128)S(1)}, f32[2,4]{1,0:T(2,128)}, u32[]{:S(2)}) copy-start(f32[2,4]{1,0:T(2,128)} %max.32) | copy-start | bytes 100
  52.8 3.2 %copy-start.8 = (bf16[512,512]{0,1:T(8,128)(2,1)S(1)}, bf16[512,512]{0,1:T(8,128)(2,1)}, u32[]{:S(2)}) copy-start(bf16[512,512]{0,1:T(8,128)(2,1)} %copy.41) | copy-start | bytes 1572868
  52.8 3.2 %copy-start.11 = (bf16[768,128]{0,1:T(8,128)(2,1)S(1)}, bf16[768,128]{0,1:T(8,128)(2,1)}, u32[]{:S(2)}) copy-start(bf16[768,128]{0,1:T(8,128)(2,1)} %copy.40) | copy-start | bytes 589828
  62.5 3.2 %copy-start.12 = (bf16[768,128]{0,1:T(8,128)(2,1)S(1)}, bf16[768,128]{0,1:T(8,128)(2,1)}, u32[]{:S(2)}) copy-start(bf16[768,128]{0,1:T(8,128)(2,1)} %copy.35) | copy-start | bytes 589828
  65.7 5.9 %copy-start.10 = (bf16[768,128]{1,0:T(8,128)(2,1)S(1)}, bf16[768,128]{1,0:T(8,128)(2,1)}, u32[]{:S(2)}) copy-start(bf16[768,128]{1,0:T(8,128)(2,1)} %get-tuple-element.12) | copy-start | bytes 589828
  71.8 8.2 %copy-start.1 = (f32[2,768,512,4]{2,1,3,0:T(8,128)S(1)}, f32[2,768,512,4]{2,1,3,0:T(8,128)}, u32[]{:S(2)}) copy-start(f32[2,768,512,4]{2,1,3,0:T(8,128)} %get-tuple-element.26) | copy-start | bytes 37748740
  87.0 3.9 %slice-start = ((s32[8,5]{0,1:T(8,128)}), s32[8,4]{0,1:T(4,128)S(1)}, s32[]{:S(2)}) async-start(s32[8,5]{0,1:T(8,128)} %copy-done.14), calls=%async_computation.4 | async-start | bytes 4096 | tf_op jit(solution)/shard_map/slice.1
  87.0 3.9 %copy-start.19 = (s32[512]{0:T(512)S(1)}, s32[512]{0:T(512)}, u32[]{:S(2)}) copy-start(s32[512]{0:T(512)} %eq.65) | copy-start | bytes 6148
  87.0 4.0 %copy-start.17 = (s32[512,1]{0,1:T(1,128)S(1)}, s32[512,1]{0,1:T(1,128)}, u32[]{:S(2)}) copy-start(s32[512,1]{0,1:T(1,128)} %mul.81) | copy-start | bytes 6148
  87.0 18.1 %all-to-all-start = ((bf16[4,256,512]{2,1,0:T(8,128)(2,1)}), bf16[4,256,512]{2,1,0:T(8,128)(2,1)S(1)}, u32[]{:S(2)}, u32[]{:S(2)}) async-start(bf16[4,256,512]{2,1,0:T(8,128)(2,1)} %bitcast.100), calls=%async_computation | async-start | bytes 2097152 | tf_op jit(solution)/shard_map/all_to_all | solution.py:112
  105.1 1.0 copy-start.5
  107.5 5.3 %copy-start.4 = (bf16[2048,2048]{1,0:T(8,128)(2,1)S(1)}, bf16[2048,2048]{1,0:T(8,128)(2,1)}, u32[]{:S(2)}) copy-start(bf16[2048,2048]{1,0:T(8,128)(2,1)} %all-gather.2.cloned.1.call-done) | copy-start | bytes 25165828
  112.9 1.2 copy-start.9
  114.1 2.2 copy-start.16
  115.3 1.0 copy-start.2
  119.9 57.8 %copy-start.23 = (bf16[1,2048,512]{2,1,0:T(8,128)(2,1)S(1)}, bf16[1,2048,512]{2,1,0:T(8,128)(2,1)}, u32[]{:S(2)}) copy-start(bf16[1,2048,512]{2,1,0:T(8,128)(2,1)} %param.21) | copy-start | bytes 6291460
  176.3 1.3 copy-start.6
  184.9 4.7 %copy-start.21 = (f32[256,2]{0,1:T(2,128)S(1)}, f32[256,2]{0,1:T(2,128)}, u32[]{:S(2)}) copy-start(f32[256,2]{0,1:T(2,128)} %param.25) | copy-start | bytes 6148
  184.9 51.8 %all-to-all-start.2 = ((bf16[8,64,2048]{2,1,0:T(8,128)(2,1)}), bf16[8,64,2048]{2,1,0:T(8,128)(2,1)}, u32[]{:S(2)}, u32[]{:S(2)}) async-start(bf16[8,64,2048]{2,1,0:T(8,128)(2,1)} %bitcast.101), calls=%async_computation.2 | async-start | bytes 4194304 | tf_op jit(solution)/shard_map/all_to_all | solution.py:155
  249.2 9.0 %copy-start.3 = (bf16[256,2048]{1,0:T(8,128)(2,1)S(1)}, bf16[256,2048]{1,0:T(8,128)(2,1)}, u32[]{:S(2)}) copy-start(bf16[256,2048]{1,0:T(8,128)(2,1)} %copy-done.2) | copy-start | bytes 3145732
  (3 other events, 2.2 us)
Sparse Core Ops, SparseCore 0:
  8.9 60.9 all-gather.1
where the time goes:
time: 267 us; the launch traced here: 266 us
  waiting for transfers between devices  59.3 us (22%)
  blocking collectives  56.4 us (21%)
  local copies, waits for them, and re-layouts  43.4 us (16%)
  matrix products  33.4 us (13%)
  other arithmetic  33.2 us (12%)
  starting transfers between devices  26.8 us (10%)
  between operations  13.8 us (5%)
    all_to_all x1, blocking collectives, per_device(): lax.all_to_all(outgoing, 'sp', split_axis=0, concat_axis=0, tiled=True)  56.4 us
    all_to_all x1, waiting for transfers between devices, per_device(): lax.all_to_all(produced.reshape(incoming.shape), 'sp', split_axis=0, conc...  46.9 us
    ppermute x3, starting transfers between devices, extended(): lax.ppermute(lax.slice_in_dim(block, block.shape[dim] - width, None, axis...  14.4 us
    all_to_all x1, waiting for transfers between devices, per_device(): lax.all_to_all(attended, 'tp', split_axis=0, concat_axis=1, tiled=True)  11.6 us
    reduce_sum x2, other arithmetic, attend(): jnp.sum(exponent, axis=3, keepdims=True) + jnp.exp(sink_col - row_top)  9.89 us
    dot_general x2, matrix products, attend(): jnp.einsum('qgrd,kgd->grqk', query_heads, key_heads, preferred_element_ty...  9.67 us
    dot_general x2, matrix products, attend(): jnp.einsum('grqk,kgd->qgrd', attn_weight, value_heads, preferred_element_...  9.31 us
    reduce_sum x1, other arithmetic, per_device(): jnp.sum(route_weights[:, :, None] * route_out.astype(jnp.float32), axis=1)  8.96 us
  transfers between devices with their start and end apart: 9, of which 2 were waited for; matrix products, arithmetic and copies ran while one was open for 24% of the time, Pallas kernels for 0%

commit v1 on v0

--- a/solution.py
+++ b/solution.py
@@ -2,6 +2,7 @@
 import jax.numpy as jnp
 from jax import lax
 from jax.sharding import PartitionSpec as P
+from jax.lax import all_to_all, psum
 
 HD = 64
 WINDOW = 128
@@ -109,7 +110,19 @@
             )
         )
     attended = jnp.concatenate(block_parts, axis=0)
-    regrouped = lax.all_to_all(attended, "tp", split_axis=0, concat_axis=1, tiled=True)
+
+    def digits_prepare(link_axis, sheet):
+        return jnp.concatenate(
+            all_to_all(
+                jnp.stack(jnp.split(sheet, psum(1, axis_name=link_axis), axis=0)),
+                split_axis=0,
+                concat_axis=0,
+                axis_name=link_axis,
+            ),
+            axis=1,
+        )
+
+    regrouped = digits_prepare("tp", attended)
     shard_rows = out_weight.shape[0]
     initial = jnp.zeros((regrouped.shape[0], out_weight.shape[1]), jnp.float32)
     running = initial

time: 267 us -> 254 us (0.951)
  matrix products: 33.4 us -> 27.5 us
  local copies, waits for them, and re-layouts: 43.4 us -> 39.7 us
  other arithmetic: 33.2 us -> 29.6 us
    dot_general x2, matrix products: 9.67 us -> 5.18 us  [attend(): jnp.einsum('qgrd,kgd->grqk', query_heads, key_heads, preferred_element_ty...]
    reduce_sum x2, other arithmetic: 9.89 us -> 6.21 us  [attend(): jnp.sum(exponent, axis=3, keepdims=True) + jnp.exp(sink_col - row_top)]
    unnamed x52 -> x48, local copies, waits for them, and re-layouts: 6 us -> 3.81 us
  transfers between devices with their start and end apart: 9 -> 9, of which waited for: 2 -> 2; matrix products, arithmetic and copies ran while one was open for 24% -> 21% of each run, Pallas kernels for 0% -> 0%
where the time goes in v1:
time: 254 us; the launch traced here: 253 us
  waiting for transfers between devices  59.3 us (23%)
  blocking collectives  56.4 us (22%)
  local copies, waits for them, and re-layouts  39.7 us (16%)
  other arithmetic  29.6 us (12%)
  matrix products  27.5 us (11%)
  starting transfers between devices  26.6 us (10%)
  between operations  13.8 us (5%)
    all_to_all x1, blocking collectives, per_device(): lax.all_to_all(outgoing, 'sp', split_axis=0, concat_axis=0, tiled=True)  56.4 us
    all_to_all x1, waiting for transfers between devices, per_device(): lax.all_to_all(produced.reshape(incoming.shape), 'sp', split_axis=0, conc...  46.9 us
    ppermute x3, starting transfers between devices, extended(): lax.ppermute(lax.slice_in_dim(block, block.shape[dim] - width, None, axis...  14.4 us
    all_to_all x1, waiting for transfers between devices, digits_prepare(): all_to_all(jnp.stack(jnp.split(sheet, psum(1, axis_name=link_axis), axis=...  11.6 us
    reduce_sum x1, other arithmetic, per_device(): jnp.sum(route_weights[:, :, None] * route_out.astype(jnp.float32), axis=1)  8.96 us
    dot_general x2, matrix products, attend(): jnp.einsum('grqk,kgd->qgrd', attn_weight, value_heads, preferred_element_...  7.89 us
    dot_general x4, matrix products, per_device(): jnp.dot(columns, weight_piece[shard_index * shard_rows:(shard_index + 1)...  7.24 us
    gather x1, local copies, waits for them, and re-layouts, per_device(): returned.reshape(-1, width)[slot_index]  7.12 us
  transfers between devices with their start and end apart: 9, of which 2 were waited for; matrix products, arithmetic and copies ran while one was open for 21% of the time, Pallas kernels for 0%

profile of v1, /device:TPU:0, one launch (start us, length us, event | category | flops | bytes accessed | tf_op | source)
XLA Modules:
  0.0 253.0 jit_solution(16243603594748408)
XLA Ops:
  8.0 4.9 %collective-permute-start.1 = (bf16[128]{0:T(256)(128)(2,1)S(1)}, bf16[128]{0:T(256)(128)(2,1)S(1)}, u32[]{:S(2)}, u32[]{:S(2)}) collective-permute-start(bf16[128]{0:T(256)(128)(2,1)S(1)} %get-tuple-element.21), channel_id=1, source_target_pairs={{0,4},{4,8},{8,12},{12,16},{16,20},{20,24},{24,28},{1,5},{5,9},{9,... | collective-permute-start | bytes 776 | tf_op jit(solution)/shard_map/ppermute | solution.py:18
  14.1 1.4 fusion.67
  15.5 4.5 %collective-permute-start.2 = (bf16[128,128]{1,0:T(8,128)(2,1)}, bf16[128,128]{1,0:T(8,128)(2,1)S(1)}, u32[]{:S(2)}, u32[]{:S(2)}) collective-permute-start(bf16[128,128]{1,0:T(8,128)(2,1)} %get-tuple-element.13), channel_id=1, source_target_pairs={{0,4},{4,8},{8,12},{12,16},{16,20},{20,24},{24,28},{1,5},{5,9},{9,... | collective-permute-start | bytes 98312 | tf_op jit(solution)/shard_map/ppermute | solution.py:18
  21.4 1.4 fusion.68
  22.8 5.0 %collective-permute-start = (bf16[128,128]{1,0:T(8,128)(2,1)}, bf16[128,128]{1,0:T(8,128)(2,1)S(1)}, u32[]{:S(2)}, u32[]{:S(2)}) collective-permute-start(bf16[128,128]{1,0:T(8,128)(2,1)} %get-tuple-element.17), channel_id=1, source_target_pairs={{0,4},{4,8},{8,12},{12,16},{16,20},{20,24},{24,28},{1,5},{5,9},{9,... | collective-permute-start | bytes 98312 | tf_op jit(solution)/shard_map/ppermute | solution.py:18
  42.4 2.4 fusion.30
  44.8 1.8 pad_maximum_fusion.3
  46.5 1.8 copy.24
  48.3 1.8 copy.28
  50.1 1.8 pad_maximum_fusion.4
  51.9 1.7 copy.23
  53.6 1.7 copy.27
  55.3 3.1 %fusion = (f32[2,4,512]{2,1,0:T(4,128)S(1)}, f32[2,768,512,4]{2,1,3,0:T(8,128)S(1)}) fusion(pred[512,768]{0,1:T(8,128)(4,1)S(1)} %get-tuple-element.34, bf16[768,2,64,1]{0,2,3,1:T(8,128)(2,1)} %bitcast.115, bf16[512,2,4,64]{0,3,2,1:T(8,128)(2,1)S(1)} %bitcast.108), kind=kOutput, calls=%fused_computation.9 | convolution fusion | flops 412086272 | bytes 13713408 | tf_op jit(solution)/shard_map/qgrd,kgd->grqk/dot_general | solution.py:44
  58.5 2.1 fusion.1
  60.6 3.1 %fusion.2 = f32[2,4,512]{2,1,0:T(4,128)S(1)} fusion(f32[2,768,512,4]{2,1,3,0:T(8,128)S(1)} %get-tuple-element.28, f32[2,4,512]{2,1,0:T(4,128)S(1)} %broadcast_maximum_fusion.1, pred[512,768]{0,1:T(8,128)(4,1)S(1)} %get-tuple-element.34), kind=kLoop, calls=%fused_computation.11 | loop fusion | flops 15724544 | bytes 13008896 | tf_op jit(solution)/shard_map/reduce_sum | solution.py:59
  63.8 3.1 %fusion.3 = f32[2,4,512]{2,1,0:T(4,128)S(1)} fusion(f32[2,768,512,4]{2,1,3,0:T(8,128)S(1)} %get-tuple-element.30, f32[2,4,512]{2,1,0:T(4,128)S(1)} %get-tuple-element.26, pred[512,768]{0,1:T(8,128)(4,1)S(1)} %get-tuple-element.33), kind=kLoop, calls=%fused_computation.12 | loop fusion | flops 15724544 | bytes 13008896 | tf_op jit(solution)/shard_map/reduce_sum | solution.py:59
  67.0 3.9 %fusion.40 = bf16[512,2,4,64]{0,3,2,1:T(8,128)(2,1)S(1)} fusion(bf16[768,2,64,1]{0,2,3,1:T(8,128)(2,1)S(1)} %bitcast.117, f32[2,768,512,4]{2,1,3,0:T(8,128)S(1)} %get-tuple-element.28, f32[2,4,512]{2,1,0:T(4,128)S(1)} %get-tuple-element.25, f32[2,4,512]{2,1,0:T(4,128)S(1)} %broadcast_maximum_fusion.1, pred[512,768]{0,1:T(8,128)(4,1)S(1)} %get-tuple-element.34), kind=kOutput, calls=%fused_computation.56 | convolution fusion | flops 421789696 | bytes 13729792 | tf_op jit(solution)/shard_map/grqk,kgd->qgrd/dot_general | solution.py:61
  71.0 3.9 %fusion.41 = bf16[512,2,4,64]{0,3,2,1:T(8,128)(2,1)S(1)} fusion(bf16[768,2,64,1]{0,2,3,1:T(8,128)(2,1)S(1)} %bitcast.116, f32[2,768,512,4]{2,1,3,0:T(8,128)S(1)} %get-tuple-element.30, f32[2,4,512]{2,1,0:T(4,128)S(1)} %exponential_add_fusion, f32[2,4,512]{2,1,0:T(4,128)S(1)} %get-tuple-element.26, pred[512,768]{0,1:T(8,128)(4,1)S(1)} %get-tuple-element.33), kind=kOutput, calls=%fused_computation.57 | convolution fusion | flops 421789696 | bytes 13729792 | tf_op jit(solution)/shard_map/grqk,kgd->qgrd/dot_general | solution.py:61
  76.2 3.7 %all-to-all-start = ((bf16[4,256,512]{1,2,0:T(8,128)(2,1)}), bf16[4,256,512]{1,2,0:T(8,128)(2,1)S(1)}, u32[]{:S(2)}, u32[]{:S(2)}) async-start(bf16[4,256,512]{1,2,0:T(8,128)(2,1)} %pad_maximum_fusion), calls=%async_computation | async-start | bytes 2097152 | tf_op jit(solution)/shard_map/all_to_all | solution.py:116
  80.0 2.4 scatter_custom_fusion
  82.5 11.6 %all-to-all-done = bf16[4,256,512]{1,2,0:T(8,128)(2,1)S(1)} async-done(((bf16[4,256,512]{1,2,0:T(8,128)(2,1)}), bf16[4,256,512]{1,2,0:T(8,128)(2,1)S(1)}, u32[]{:S(2)}, u32[]{:S(2)}) %all-to-all-start) | async-done | bytes 1048608 | tf_op jit(solution)/shard_map/all_to_all | solution.py:116
  94.1 2.5 fusion.12
  96.6 2.9 %fusion.13 = f32[256,2048]{1,0:T(8,128)S(1)} fusion(bf16[2048,2048]{1,0:T(8,128)(2,1)} %all-gather.2.cloned.1.call-done, bf16[256,2048]{0,1:T(8,128)(2,1)S(1)} %bitcast.102), kind=kOutput, calls=%fused_computation.31 | convolution fusion | flops 537919488 | bytes 4456448 | tf_op jit(solution)/shard_map/dot_general | solution.py:132
  103.2 3.3 %gather_fusion = bf16[512,2048]{1,0:T(8,128)(2,1)} fusion(bf16[256,2048]{1,0:T(8,128)(2,1)S(1)} %fusion.17, s32[1024]{0:T(1024)S(1)} %pad_clamp_fusion.1), kind=kCustom, calls=%fused_computation | custom fusion | bytes 4196352 | tf_op jit(solution)/shard_map/gather | solution.py:159
  106.5 56.4 %all_to_all.15 = bf16[8,64,2048]{2,1,0:T(8,128)(2,1)S(1)} all-to-all(bf16[8,64,2048]{2,1,0:T(8,128)(2,1)} %bitcast.100), channel_id=1, replica_groups=mesh['sp'=8,'tp'=4] {'sp'}, dimensions={0} | all-to-all | bytes 4194304 | tf_op jit(solution)/shard_map/all_to_all | solution.py:160
  162.9 1.3 copy-done.4
  165.5 6.0 %convolution_convert_fusion = bf16[512,2048]{1,0:T(8,128)(2,1)} fusion(bf16[1,512,2048]{2,1,0:T(8,128)(2,1)S(1)} %copy-done, bf16[512,2048]{1,0:T(8,128)(2,1)} %bitcast.107, bf16[1,2048,512]{2,1,0:T(8,128)(2,1)} %param.22, f32[512,512]{1,0:T(8,128)S(1)} %fusion.26), kind=kOutput, calls=%fused_computation.19 | convolution fusion | flops 2150105088 | bytes 9437184 | tf_op jit(solution)/shard_map/dot_general | solution.py:165
  171.5 4.7 %all-to-all-start.2 = ((bf16[8,64,2048]{2,1,0:T(8,128)(2,1)}), bf16[8,64,2048]{2,1,0:T(8,128)(2,1)}, u32[]{:S(2)}, u32[]{:S(2)}) async-start(bf16[8,64,2048]{2,1,0:T(8,128)(2,1)} %bitcast.105), calls=%async_computation.2 | async-start | bytes 4194304 | tf_op jit(solution)/shard_map/all_to_all | solution.py:168
  176.4 46.9 %all-to-all-done.2 = bf16[8,64,2048]{2,1,0:T(8,128)(2,1)} async-done(((bf16[8,64,2048]{2,1,0:T(8,128)(2,1)}), bf16[8,64,2048]{2,1,0:T(8,128)(2,1)}, u32[]{:S(2)}, u32[]{:S(2)}) %all-to-all-start.2) | async-done | bytes 2097184 | tf_op jit(solution)/shard_map/all_to_all | solution.py:168
  223.3 7.1 %gather_fusion.1 = bf16[512,2048]{1,0:T(8,128)(2,1)} fusion(bf16[512,2048]{1,0:T(8,128)(2,1)} %bitcast.35, s32[1024]{0:T(1024)S(1)} %pad_clamp_fusion), kind=kCustom, calls=%fused_computation.1 | custom fusion | bytes 4196352 | tf_op jit(solution)/shard_map/gather | solution.py:171
  230.4 5.5 %reshape.319 = f32[256,2,2048]{2,1,0:T(2,128)} reshape(bf16[512,2048]{1,0:T(8,128)(2,1)} %gather_fusion.1) | data formatting | bytes 6291456 | tf_op jit(solution)/shard_map/convert_element_type | solution.py:172
  235.9 9.0 %multiply_reduce_fusion = f32[256,2048]{1,0:T(8,128)S(1)} fusion(f32[256,2,2048]{2,1,0:T(2,128)} %reshape.319, f32[256,2]{1,0:T(8,128)S(1)} %copy.31), kind=kLoop, calls=%fused_computation.15 | loop fusion | flops 1572864 | bytes 6293504 | tf_op jit(solution)/shard_map/reduce_sum | solution.py:172
  (101 shorter events, 26.5 us)
Async XLA Ops:
  6.5 159.0 %copy-start = (bf16[1,512,2048]{2,1,0:T(8,128)(2,1)S(1)}, bf16[1,512,2048]{2,1,0:T(8,128)(2,1)}, u32[]{:S(2)}) copy-start(bf16[1,512,2048]{2,1,0:T(8,128)(2,1)} %param.23) | copy-start | bytes 6291460
  6.5 0.8 copy-start.18
  6.5 21.2 %copy-start.15 = (s32[256,2]{0,1:T(2,128)S(1)}, s32[256,2]{0,1:T(2,128)}, u32[]{:S(2)}) copy-start(s32[256,2]{0,1:T(2,128)} %param.24) | copy-start | bytes 6148
  6.5 87.6 %all-gather.2.cloned.1.call-start = ((), (), s32[]{:S(2)}) async-start(), calls=%async_computation.3 | async-start | bytes 10485760 | tf_op jit(solution)/shard_map/all_gather | solution.py:129
  7.4 23.7 %copy-start.22 = (f32[8]{0:T(128)S(1)}, f32[8]{0:T(128)}, u32[]{:S(2)}) copy-start(f32[8]{0:T(128)} %param.17) | copy-start | bytes 100
  7.4 29.9 %copy-start.11 = (bf16[1024]{0:T(1024)(128)(2,1)}, bf16[1024]{0:T(1024)(128)(2,1)S(1)}, u32[]{:S(2)}) copy-start(bf16[1024]{0:T(1024)(128)(2,1)S(1)} %convert_element_type.80) | copy-start | bytes 6148
  8.0 31.8 %collective-permute-start.1 = (bf16[128]{0:T(256)(128)(2,1)S(1)}, bf16[128]{0:T(256)(128)(2,1)S(1)}, u32[]{:S(2)}, u32[]{:S(2)}) collective-permute-start(bf16[128]{0:T(256)(128)(2,1)S(1)} %get-tuple-element.21), channel_id=1, source_target_pairs={{0,4},{4,8},{8,12},{12,16},{16,20},{20,24},{24,28},{1,5},{5,9},{9,... | collective-permute-start | bytes 776 | tf_op jit(solution)/shard_map/ppermute | solution.py:18
  12.8 28.8 %collective-permute-start.4 = (bf16[128]{0:T(256)(128)(2,1)}, bf16[128]{0:T(256)(128)(2,1)}, u32[]{:S(2)}, u32[]{:S(2)}) collective-permute-start(bf16[128]{0:T(256)(128)(2,1)} %get-tuple-element.22), channel_id=1, source_target_pairs={{4,0},{8,4},{12,8},{16,12},{20,16},{24,20},{28,24},{5,1},{9,5},{13... | collective-permute-start | bytes 776 | tf_op jit(solution)/shard_map/ppermute | solution.py:21
  15.5 29.2 %collective-permute-start.2 = (bf16[128,128]{1,0:T(8,128)(2,1)}, bf16[128,128]{1,0:T(8,128)(2,1)S(1)}, u32[]{:S(2)}, u32[]{:S(2)}) collective-permute-start(bf16[128,128]{1,0:T(8,128)(2,1)} %get-tuple-element.13), channel_id=1, source_target_pairs={{0,4},{4,8},{8,12},{12,16},{16,20},{20,24},{24,28},{1,5},{5,9},{9,... | collective-permute-start | bytes 98312 | tf_op jit(solution)/shard_map/ppermute | solution.py:18
  20.1 24.7 %collective-permute-start.5 = (bf16[128,128]{1,0:T(8,128)(2,1)}, bf16[128,128]{1,0:T(8,128)(2,1)S(1)}, u32[]{:S(2)}, u32[]{:S(2)}) collective-permute-start(bf16[128,128]{1,0:T(8,128)(2,1)} %get-tuple-element.14), channel_id=1, source_target_pairs={{4,0},{8,4},{12,8},{16,12},{20,16},{24,20},{28,24},{5,1},{9,5},{13... | collective-permute-start | bytes 98312 | tf_op jit(solution)/shard_map/ppermute | solution.py:21
  22.8 27.3 %collective-permute-start = (bf16[128,128]{1,0:T(8,128)(2,1)}, bf16[128,128]{1,0:T(8,128)(2,1)S(1)}, u32[]{:S(2)}, u32[]{:S(2)}) collective-permute-start(bf16[128,128]{1,0:T(8,128)(2,1)} %get-tuple-element.17), channel_id=1, source_target_pairs={{0,4},{4,8},{8,12},{12,16},{16,20},{20,24},{24,28},{1,5},{5,9},{9,... | collective-permute-start | bytes 98312 | tf_op jit(solution)/shard_map/ppermute | solution.py:18
  38.3 17.1 %copy-start.5 = (bf16[512,512]{0,1:T(8,128)(2,1)S(1)}, bf16[512,512]{0,1:T(8,128)(2,1)}, u32[]{:S(2)}) copy-start(bf16[512,512]{0,1:T(8,128)(2,1)} %copy.25) | copy-start | bytes 1572868
  39.7 0.6 copy-start.20
  40.3 9.8 %collective-permute-start.3 = (bf16[128,128]{1,0:T(8,128)(2,1)}, bf16[128,128]{1,0:T(8,128)(2,1)S(1)}, u32[]{:S(2)}, u32[]{:S(2)}) collective-permute-start(bf16[128,128]{1,0:T(8,128)(2,1)} %get-tuple-element.18), channel_id=1, source_target_pairs={{4,0},{8,4},{12,8},{16,12},{20,16},{24,20},{28,24},{5,1},{9,5},{13... | collective-permute-start | bytes 98312 | tf_op jit(solution)/shard_map/ppermute | solution.py:21
  55.3 3.1 %copy-start.12 = (f32[2,4]{1,0:T(2,128)S(1)}, f32[2,4]{1,0:T(2,128)}, u32[]{:S(2)}) copy-start(f32[2,4]{1,0:T(2,128)} %max.32) | copy-start | bytes 100
  55.3 3.2 %copy-start.6 = (bf16[512,512]{0,1:T(8,128)(2,1)S(1)}, bf16[512,512]{0,1:T(8,128)(2,1)}, u32[]{:S(2)}) copy-start(bf16[512,512]{0,1:T(8,128)(2,1)} %copy.29) | copy-start | bytes 1572868
  55.3 3.2 %copy-start.8 = (bf16[768,128]{0,1:T(8,128)(2,1)S(1)}, bf16[768,128]{0,1:T(8,128)(2,1)}, u32[]{:S(2)}) copy-start(bf16[768,128]{0,1:T(8,128)(2,1)} %copy.28) | copy-start | bytes 589828
  63.8 3.2 %copy-start.10 = (bf16[768,128]{0,1:T(8,128)(2,1)S(1)}, bf16[768,128]{0,1:T(8,128)(2,1)}, u32[]{:S(2)}) copy-start(bf16[768,128]{0,1:T(8,128)(2,1)} %copy.23) | copy-start | bytes 589828
  67.0 4.0 %copy-start.9 = (bf16[768,128]{0,1:T(8,128)(2,1)S(1)}, bf16[768,128]{0,1:T(8,128)(2,1)}, u32[]{:S(2)}) copy-start(bf16[768,128]{0,1:T(8,128)(2,1)} %copy.27) | copy-start | bytes 589828
  75.1 4.9 %copy-start.16 = (s32[512]{0:T(512)S(1)}, s32[512]{0:T(512)}, u32[]{:S(2)}) copy-start(s32[512]{0:T(512)} %eq.65) | copy-start | bytes 6148
  75.1 4.9 %copy-start.17 = (s32[8,4]{0,1:T(4,128)S(1)}, s32[8,4]{0,1:T(4,128)}, u32[]{:S(2)}) copy-start(s32[8,4]{0,1:T(4,128)} %slice.97) | copy-start | bytes 388
  75.1 4.9 %copy-start.14 = (s32[512,1]{0,1:T(1,128)S(1)}, s32[512,1]{0,1:T(1,128)}, u32[]{:S(2)}) copy-start(s32[512,1]{0,1:T(1,128)} %mul.81) | copy-start | bytes 6148
  76.2 17.9 %all-to-all-start = ((bf16[4,256,512]{1,2,0:T(8,128)(2,1)}), bf16[4,256,512]{1,2,0:T(8,128)(2,1)S(1)}, u32[]{:S(2)}, u32[]{:S(2)}) async-start(bf16[4,256,512]{1,2,0:T(8,128)(2,1)} %pad_maximum_fusion), calls=%async_computation | async-start | bytes 2097152 | tf_op jit(solution)/shard_map/all_to_all | solution.py:116
  94.1 5.3 %copy-start.3 = (bf16[2048,2048]{1,0:T(8,128)(2,1)S(1)}, bf16[2048,2048]{1,0:T(8,128)(2,1)}, u32[]{:S(2)}) copy-start(bf16[2048,2048]{1,0:T(8,128)(2,1)} %all-gather.2.cloned.1.call-done) | copy-start | bytes 25165828
  99.5 1.2 copy-start.7
  100.7 2.2 copy-start.13
  101.9 1.0 copy-start.1
  106.5 57.8 %copy-start.21 = (bf16[1,2048,512]{2,1,0:T(8,128)(2,1)S(1)}, bf16[1,2048,512]{2,1,0:T(8,128)(2,1)}, u32[]{:S(2)}) copy-start(bf16[1,2048,512]{2,1,0:T(8,128)(2,1)} %param.21) | copy-start | bytes 6291460
  162.9 1.3 copy-start.4
  171.5 4.7 %copy-start.19 = (f32[256,2]{0,1:T(2,128)S(1)}, f32[256,2]{0,1:T(2,128)}, u32[]{:S(2)}) copy-start(f32[256,2]{0,1:T(2,128)} %param.25) | copy-start | bytes 6148
  171.5 51.8 %all-to-all-start.2 = ((bf16[8,64,2048]{2,1,0:T(8,128)(2,1)}), bf16[8,64,2048]{2,1,0:T(8,128)(2,1)}, u32[]{:S(2)}, u32[]{:S(2)}) async-start(bf16[8,64,2048]{2,1,0:T(8,128)(2,1)} %bitcast.105), calls=%async_computation.2 | async-start | bytes 4194304 | tf_op jit(solution)/shard_map/all_to_all | solution.py:168
  235.9 9.0 %copy-start.2 = (bf16[256,2048]{1,0:T(8,128)(2,1)S(1)}, bf16[256,2048]{1,0:T(8,128)(2,1)}, u32[]{:S(2)}) copy-start(bf16[256,2048]{1,0:T(8,128)(2,1)} %copy-done.1) | copy-start | bytes 3145732
Sparse Core Ops, SparseCore 0:
  8.9 60.9 all-gather.1
